TPU v7x, 32 devices: a whole 2x2x4 slice. The times are simulated.
32 devices in a mesh: sp: 8 (over z, x), tp: 4 (over y, core).
Axes of the slice: x: 2, y: 2, z: 4, core: 2. Of those that a mesh axis runs over, the one named last changes fastest.
Arguments:
- residual: bfloat16 [1536, 2048], P(('sp', 'tp')), may hold values from -6 to 6
- query_a: bfloat16 [1536, 1536], P('sp', 'tp'), may hold values from -600 to 600
- query_b: bfloat16 [1536, 2560], P('sp', 'tp'), may hold values from -600 to 600
- latents: bfloat16 [1536, 512], P('sp'), may hold values from -6 to 6
- rope_key: bfloat16 [1536, 32], P('sp'), may hold values from -6 to 6
- key_up_a: bfloat16 [512, 1024], P(None, 'tp'), may hold values from -0.25 to 0.25
- value_up_a: bfloat16 [512, 1024], P(None, 'tp'), may hold values from -0.25 to 0.25
- key_up_b: bfloat16 [512, 2048], P(None, 'tp'), may hold values from -0.25 to 0.25
- value_up_b: bfloat16 [512, 2048], P(None, 'tp'), may hold values from -0.25 to 0.25
- out_proj_a: bfloat16 [1024, 2048], P('tp'), may hold values from -1.5 to 1.5
- out_proj_b: bfloat16 [2048, 2048], P('tp'), may hold values from -1.5 to 1.5
- norm_gain: float32 [2048], replicated, may hold values from 0.1 to 1.9
- routes: int32 [1536, 2], P('sp'), may hold values from 0 to 7, all different within a row; in each aligned block of 192 rows (0 to 191, 192 to 383, ...) at most 72 rows name the same one
- route_weights: float32 [1536, 2], P('sp'), may hold values from 0.2 to 1
- shared_gate: bfloat16 [2048, 2048], P(None, 'tp'), may hold values from -0.125 to 0.125
- shared_up: bfloat16 [2048, 2048], P(None, 'tp'), may hold values from -0.125 to 0.125
- shared_down: bfloat16 [2048, 2048], P('tp'), may hold values from -0.125 to 0.125
- expert_gate: bfloat16 [8, 2048, 2048], P('sp', None, 'tp'), may hold values from -0.125 to 0.125
- expert_up: bfloat16 [8, 2048, 2048], P('sp', None, 'tp'), may hold values from -0.125 to 0.125
- expert_down: bfloat16 [8, 2048, 2048], P('sp', 'tp'), may hold values from -0.125 to 0.125
Outputs:
- layer_out: bfloat16 [1536, 2048], P(('sp', 'tp'))
Inputs may be any that keep to these rules, and one draw needn't show every extreme that they name: `routes`: in each aligned block of 192 rows, no expert is named by more than 72 rows, a bound that some block reaches; a row names 2 different experts.
All inputs are finite; a program needn't handle non-finite values.
Results may differ from a plain program's by a relative error of at most 0.022.
The roundings to bfloat16 on the way count: a program that leaves them out, or rounds other values in their place, can miss the bound.
Values may be sent and summed in bfloat16 or wider, within the bound.
A program may use at most 64 MiB of HBM per device.

v0:
```python
import jax
import jax.numpy as jnp
from jax import lax
from jax.sharding import PartitionSpec as P

DA = 64
VA = 64
DB = 128
VB = 128
ROPE = 32


theta_base = 10000.0
norm_eps = 1e-06
very_low = -1e30


def tables(positions, width):
    half = width // 2
    freqs = theta_base ** (-(2.0 * jnp.arange(half, dtype=jnp.float32)) / width)
    angles = positions.astype(jnp.float32)[:, None] * freqs[None, :]
    return (jnp.cos(angles), jnp.sin(angles))


def rotate(values, cosine, sine):
    half = values.shape[-1] // 2
    first = values[..., :half].astype(jnp.float32)
    second = values[..., half:].astype(jnp.float32)
    turned = jnp.concatenate(
        [first * cosine - second * sine, first * sine + second * cosine], axis=-1
    )
    return turned.astype(jnp.bfloat16)


def group_update(state, queries_nope, queries_rope, keys, values, rot_piece, mask, scale):
    top, total, weighted = state
    scores = jnp.einsum("qhd,khd->hqk", queries_nope, keys, preferred_element_type=jnp.float32)
    scores = scores + jnp.einsum(
        "qhr,kr->hqk", queries_rope, rot_piece, preferred_element_type=jnp.float32
    )
    scores = jnp.where(mask[None], scores * scale, very_low)
    new_top = jnp.maximum(top, jnp.max(scores, axis=-1))
    expo = jnp.where(mask[None], jnp.exp(scores - new_top[..., None]), 0.0)
    total = jnp.sum(expo, axis=-1)
    weighted = jnp.einsum(
        "hqk,khv->hqv", expo.astype(jnp.bfloat16), values, preferred_element_type=jnp.float32
    )
    return (new_top, total, weighted)


def empty_state(heads, rows, vsize):
    return (
        jnp.full((heads, rows), very_low, jnp.float32),
        jnp.zeros((heads, rows), jnp.float32),
        jnp.zeros((heads, rows, vsize), jnp.float32),
    )


def shards(
    residual,
    query_a,
    query_b,
    latents,
    rope_key,
    key_up_a,
    value_up_a,
    key_up_b,
    value_up_b,
    out_proj_a,
    out_proj_b,
    norm_gain,
    routes,
    route_weights,
    shared_gate,
    shared_up,
    shared_down,
    expert_gate,
    expert_up,
    expert_down,
):
    tok = query_a.shape[0]
    heads_a = key_up_a.shape[1] // DA
    heads_b = key_up_b.shape[1] // DB
    first_row = lax.axis_index("sp") * tok
    last_row = first_row + tok
    query_pos = first_row + jnp.arange(tok, dtype=jnp.int32)
    cosine, sine = tables(query_pos, ROPE)
    rot_key = rotate(rope_key, cosine, sine)
    shaped_a = query_a.reshape(tok, heads_a, DA + ROPE)
    shaped_b = query_b.reshape(tok, heads_b, DB + ROPE)
    nope_a = shaped_a[..., :DA]
    nope_b = shaped_b[..., :DB]
    turned_a = rotate(shaped_a[..., DA:], cosine[:, None, :], sine[:, None, :])
    turned_b = rotate(shaped_b[..., DB:], cosine[:, None, :], sine[:, None, :])
    scale_a = (DA + ROPE) ** (-0.5)
    scale_b = (DB + ROPE) ** (-0.5)

    def attend(state, keys_a, values_a, keys_b, values_b, rot_piece, key_pos):
        count = keys_a.shape[0]
        mask = key_pos[None, :] <= query_pos[:, None]
        state_a = group_update(
            state[0],
            nope_a,
            turned_a,
            keys_a.reshape(count, heads_a, DA),
            values_a.reshape(count, heads_a, VA),
            rot_piece,
            mask,
            scale_a,
        )
        state_b = group_update(
            state[1],
            nope_b,
            turned_b,
            keys_b.reshape(count, heads_b, DB),
            values_b.reshape(count, heads_b, VB),
            rot_piece,
            mask,
            scale_b,
        )
        return (state_a, state_b)

    def project_latents(lat_rows):
        keys_a = jnp.dot(lat_rows, key_up_a, preferred_element_type=jnp.float32).astype(
            jnp.bfloat16
        )
        values_a = jnp.dot(lat_rows, value_up_a, preferred_element_type=jnp.float32).astype(
            jnp.bfloat16
        )
        keys_b = jnp.dot(lat_rows, key_up_b, preferred_element_type=jnp.float32).astype(
            jnp.bfloat16
        )
        values_b = jnp.dot(lat_rows, value_up_b, preferred_element_type=jnp.float32).astype(
            jnp.bfloat16
        )
        return (keys_a, values_a, keys_b, values_b)

    start_state = (empty_state(heads_a, tok, VA), empty_state(heads_b, tok, VB))
    lat_rows = lax.all_gather(latents, "sp", axis=0, tiled=True)
    rot_piece = lax.all_gather(rot_key, "sp", axis=0, tiled=True)
    key_pos = jnp.arange(lat_rows.shape[0], dtype=jnp.int32)

    def compute(inner):
        keys_a, values_a, keys_b, values_b = project_latents(lat_rows)
        return attend(inner, keys_a, values_a, keys_b, values_b, rot_piece, key_pos)

    state = lax.cond(jnp.int32(0) < last_row, compute, lambda inner: inner, start_state)
    heads_out_a = (state[0][2] / state[0][1][..., None]).astype(jnp.bfloat16)
    heads_out_b = (state[1][2] / state[1][1][..., None]).astype(jnp.bfloat16)
    proj_a = out_proj_a.reshape(heads_a, VA, out_proj_a.shape[1])
    proj_b = out_proj_b.reshape(heads_b, VB, out_proj_b.shape[1])
    term = jnp.einsum("hqv,hvd->qd", heads_out_a, proj_a, preferred_element_type=jnp.float32)
    mixed = lax.psum_scatter(
        (
            term
            + jnp.einsum("hqv,hvd->qd", heads_out_b, proj_b, preferred_element_type=jnp.float32)
        ).astype(jnp.bfloat16),
        "tp",
        scatter_dimension=0,
        tiled=True,
    ).astype(jnp.float32)
    hidden_state = (residual.astype(jnp.float32) + mixed).astype(jnp.bfloat16)
    wide = hidden_state.astype(jnp.float32)
    normed = (
        wide * lax.rsqrt(jnp.mean(wide * wide, axis=-1, keepdims=True) + norm_eps) * norm_gain
    ).astype(jnp.bfloat16)
    whole_rows = lax.all_gather(normed, "tp", axis=0, tiled=True)
    shared_act = (
        jax.nn.silu(jnp.dot(whole_rows, shared_gate, preferred_element_type=jnp.float32))
        * jnp.dot(whole_rows, shared_up, preferred_element_type=jnp.float32)
    ).astype(jnp.bfloat16)
    experts = lax.axis_size("sp")
    topk = routes.shape[1]
    capacity = max(2, 3 * tok * topk // (2 * experts))
    flat = routes.reshape(-1)
    onehot = (flat[:, None] == jnp.arange(experts, dtype=jnp.int32)[None, :]).astype(jnp.int32)
    before = jnp.cumsum(onehot, axis=0) - onehot
    rank = jnp.sum(before * onehot, axis=1)
    slots = (flat * capacity + rank).reshape(tok, topk)
    placing = jnp.sum(
        (
            slots[:, :, None] == jnp.arange(experts * capacity, dtype=jnp.int32)[None, None, :]
        ).astype(jnp.bfloat16),
        axis=1,
    )
    outgoing = jnp.einsum(
        "rs,rd->sd", placing, whole_rows, preferred_element_type=jnp.float32
    ).astype(jnp.bfloat16)
    outgoing = outgoing.reshape(experts, capacity, whole_rows.shape[1])
    gate_w = expert_gate[0]
    up_w = expert_up[0]
    down_w = expert_down[0]
    arrived = lax.all_to_all(outgoing, "sp", split_axis=0, concat_axis=0, tiled=True)
    sources, items, width = arrived.shape
    rows_in = arrived.reshape(sources * items, width)
    act = (
        jax.nn.silu(jnp.dot(rows_in, gate_w, preferred_element_type=jnp.float32))
        * jnp.dot(rows_in, up_w, preferred_element_type=jnp.float32)
    ).astype(jnp.bfloat16)
    part = jnp.dot(act, down_w, preferred_element_type=jnp.float32).astype(jnp.bfloat16)
    back = lax.all_to_all(
        part.reshape(sources, items, down_w.shape[1]), "sp", split_axis=0, concat_axis=0, tiled=True
    )
    back_flat = back.reshape(experts * capacity, back.shape[2])
    term = jnp.dot(shared_act, shared_down, preferred_element_type=jnp.float32)
    picked = jnp.take(back_flat, slots, axis=0).astype(jnp.float32)
    moe = lax.psum_scatter(
        (term + jnp.sum(picked * route_weights[..., None], axis=1)).astype(jnp.bfloat16),
        "tp",
        scatter_dimension=0,
        tiled=True,
    ).astype(jnp.float32)
    return (hidden_state.astype(jnp.float32) + moe).astype(jnp.bfloat16)


def solution(mesh):
    placed = (
        P(("sp", "tp"), None),
        P("sp", "tp"),
        P("sp", "tp"),
        P("sp", None),
        P("sp", None),
        P(None, "tp"),
        P(None, "tp"),
        P(None, "tp"),
        P(None, "tp"),
        P("tp", None),
        P("tp", None),
        P(),
        P("sp", None),
        P("sp", None),
        P(None, "tp"),
        P(None, "tp"),
        P("tp", None),
        P("sp", None, "tp"),
        P("sp", None, "tp"),
        P("sp", "tp", None),
    )
    return jax.shard_map(
        shards, mesh=mesh, in_specs=placed, out_specs=P(("sp", "tp"), None), check_vma=False
    )
```

profile of v0, /device:TPU:0, one launch (start us, length us, event | category | flops | bytes accessed | tf_op | source)
XLA Modules:
  0.0 296.8 jit_solution(13761831657723779826)
XLA Ops:
  7.3 1.0 copy.80
  8.4 1.1 copy.82
  10.4 32.5 %all-gather = bf16[8,192,32]{1,2,0:T(8,128)(2,1)S(1)} all-gather(bf16[1,192,32]{1,2,0:T(8,128)(2,1)S(1)} %maximum_bitcast_fusion), channel_id=1, replica_groups=mesh['sp'=8,'tp'=4] {'sp'}, dimensions={0}, use_global_device_ids=true | all-gather | bytes 110592 | tf_op jit(solution)/shard_map/all_gather | solution.py:140
  43.0 13.4 %all-gather.3.cloned.1.call-done = bf16[1536,512]{1,0:T(8,128)(2,1)} async-done(((bf16[192,512]{1,0:T(8,128)(2,1)}), bf16[1536,512]{1,0:T(8,128)(2,1)}) %all-gather.3.cloned.1.call-update) | async-done | bytes 1572880 | tf_op jit(solution)/shard_map/all_gather | solution.py:139
  57.0 19.7 %conditional.1 = (f32[4,192]{1,0:T(4,128)S(1)}, f32[4,192,64]{1,2,0:T(8,128)S(1)}, f32[4,192]{1,0:T(4,128)S(1)}, f32[4,192,128]{2,1,0:T(8,128)S(1)}) conditional(s32[]{:T(128)} %convert_element_type.111, () %tuple.13, (s32[1536]{0:T(1024)S(1)}, s32[]{:T(128)}, s32[192]{0:T(256)}, bf16[1536,512]{1,0:T(8,128)(2,1)}, bf16[512,256]{1,0:T(8,128)(2,1)}, ...), branch_computations={%region_0.0_spmd, %region_1.6_spmd} | conditional | flops 3499129600 | bytes 87277032 | solution.py:147
  57.3 2.9 fusion.20
  60.2 2.2 convolution_convert_fusion.1
  62.9 4.1 %fusion.75 = (f32[4,192]{1,0:T(4,128)S(1)}, f32[4,192,1536]{2,1,0:T(8,128)S(1)}) fusion(f32[1536,192,4]{0,1,2:T(8,128)} %fusion.20, bf16[1536,4,128]{0,2,1:T(8,128)(2,1)} %bitcast.102, bf16[192,4,160]{2,0,1:T(8,128)(2,1)S(1)} %copy.83, pred[192,1536]{1,0:T(8,128)(4,1)S(1)} %broadcast_compare_fusion), kind=kOutput, calls=%fused_computation.123 | convolution fusion | flops 306707712 | bytes 11504640 | tf_op jit(solution)/shard_map/cond/branch_1_fun/qhd,khd->hqk/dot_general | solution.py:37
  69.1 1.6 fusion.76
  70.7 2.3 fusion.7
  73.7 1.1 fusion.10
  74.8 1.0 convolution_convert_fusion
  75.8 0.9 fusion.8
  76.7 1.6 convolution_bitcast_fusion
  78.4 1.6 fusion.27
  82.1 19.8 %reduce-scatter.3.cloned.1.call-done = bf16[48,2048]{1,0:T(8,128)(2,1)} async-done(((bf16[192,2048]{1,0:T(8,128)(2,1)}), bf16[48,2048]{1,0:T(8,128)(2,1)}) %reduce-scatter.3.cloned.1.call-update) | async-done | bytes 196624 | tf_op jit(solution)/shard_map/reduce_scatter | solution.py:153
  101.9 1.1 fusion.46
  103.0 1.0 fusion.48
  104.1 8.2 %all_gather.11 = bf16[192,2048]{1,0:T(8,128)(2,1)S(1)} all-gather(bf16[48,2048]{1,0:T(8,128)(2,1)S(1)} %fusion.48), channel_id=1, replica_groups=mesh['sp'=8,'tp'=4] {'tp'}, dimensions={0}, use_global_device_ids=true | all-gather | bytes 983040 | tf_op jit(solution)/shard_map/all_gather | solution.py:167
  113.1 59.7 %all_to_all.10 = bf16[8,72,2048]{2,1,0:T(8,128)(2,1)S(1)} all-to-all(bf16[8,72,2048]{2,1,0:T(8,128)(2,1)S(1)} %bitcast.95), channel_id=1, replica_groups=mesh['sp'=8,'tp'=4] {'sp'}, dimensions={0} | all-to-all | bytes 4718592 | tf_op jit(solution)/shard_map/all_to_all | solution.py:193
  172.9 1.4 copy-done.3
  174.3 2.4 fusion.32
  176.7 7.4 %convolution_convert_fusion.4 = bf16[576,2048]{1,0:T(8,128)(2,1)} fusion(bf16[1,512,2048]{2,1,0:T(8,128)(2,1)} %param.41, bf16[576,2048]{1,0:T(8,128)(2,1)} %bitcast.99, bf16[1,2048,512]{2,1,0:T(8,128)(2,1)} %param.40, f32[576,512]{1,0:T(8,128)} %fusion.32), kind=kOutput, calls=%fused_computation.39 | convolution fusion | flops 2418868224 | bytes 10092544 | tf_op jit(solution)/shard_map/dot_general | solution.py:200
  184.1 4.5 %all-to-all-start.1 = ((bf16[8,72,2048]{2,1,0:T(8,128)(2,1)}), bf16[8,72,2048]{2,1,0:T(8,128)(2,1)}, u32[]{:S(2)}, u32[]{:S(2)}) async-start(bf16[8,72,2048]{2,1,0:T(8,128)(2,1)} %bitcast.97), calls=%async_computation.2 | async-start | bytes 4718592 | tf_op jit(solution)/shard_map/all_to_all | solution.py:201
  189.3 2.9 fusion.77
  192.2 49.9 %all-to-all-done.1 = bf16[8,72,2048]{2,1,0:T(8,128)(2,1)} async-done(((bf16[8,72,2048]{2,1,0:T(8,128)(2,1)}), bf16[8,72,2048]{2,1,0:T(8,128)(2,1)}, u32[]{:S(2)}, u32[]{:S(2)}) %all-to-all-start.1) | async-done | bytes 2359328 | tf_op jit(solution)/shard_map/all_to_all | solution.py:201
  242.1 7.0 %gather_fusion = bf16[384,2048]{1,0:T(8,128)(2,1)} fusion(bf16[576,2048]{1,0:T(8,128)(2,1)} %bitcast.24, s32[1024]{0:T(1024)S(1)} %pad_clamp_fusion), kind=kCustom, calls=%fused_computation | custom fusion | bytes 3147264 | tf_op jit(solution)/shard_map/jit(_take)/gather | solution.py:206
  249.2 3.8 %reshape.181 = bf16[192,2,2048]{2,1,0:T(2,128)(2,1)} reshape(bf16[384,2048]{1,0:T(8,128)(2,1)} %gather_fusion) | data formatting | bytes 3145728 | tf_op jit(solution)/shard_map/jit(_take)/gather | solution.py:206
  252.9 8.7 %multiply_reduce_fusion = f32[192,2048]{1,0:T(8,128)} fusion(bf16[192,2,2048]{2,1,0:T(2,128)(2,1)} %reshape.181, pred[192,2]{1,0:T(8,128)(4,1)S(1)} %copy.87, f32[192,2]{1,0:T(8,128)S(1)} %copy.89), kind=kLoop, calls=%fused_computation.37 | loop fusion | flops 2752512 | bytes 3147648 | tf_op jit(solution)/shard_map/reduce_sum | solution.py:208
  261.7 4.8 %fusion.28 = bf16[192,2048]{1,0:T(8,128)(2,1)} fusion(f32[192,2048]{1,0:T(8,128)} %multiply_reduce_fusion, bf16[512,2048]{1,0:T(8,128)(2,1)} %param.38, bf16[192,2048]{1,0:T(8,128)(2,1)S(1)} %all_gather.11, bf16[2048,512]{1,0:T(8,128)(2,1)} %param.37, f32[192,512]{1,0:T(8,128)} %fusion.77), kind=kOutput, calls=%fused_computation.46 | convolution fusion | flops 806682624 | bytes 7733248 | tf_op jit(solution)/shard_map/dot_general | solution.py:205
  266.5 22.0 %reduce-scatter.5.cloned.1.call-done = bf16[48,2048]{1,0:T(8,128)(2,1)} async-done(((bf16[192,2048]{1,0:T(8,128)(2,1)}), bf16[48,2048]{1,0:T(8,128)(2,1)}) %reduce-scatter.5.cloned.1.call-update) | async-done | bytes 196624 | tf_op jit(solution)/shard_map/reduce_scatter | solution.py:207
  288.6 1.7 fusion.49
  (72 shorter events, 9.1 us)
Async XLA Ops:
  6.5 71.8 %copy-start = (bf16[512,2048]{1,0:T(8,128)(2,1)S(1)}, bf16[512,2048]{1,0:T(8,128)(2,1)}, u32[]{:S(2)}) copy-start(bf16[512,2048]{1,0:T(8,128)(2,1)} %param.32) | copy-start | bytes 6291460
  6.5 49.9 %all-gather.3.cloned.1.call-start = ((), (), s32[]{:S(2)}) async-start(), calls=%async_computation.4 | async-start | bytes 1769472 | tf_op jit(solution)/shard_map/all_gather | solution.py:139
  7.3 94.6 %reduce-scatter.3.cloned.1.call-start = ((), (), s32[]{:S(2)}) async-start(), calls=%async_computation.5 | async-start | bytes 983040 | tf_op jit(solution)/shard_map/reduce_scatter | solution.py:153
  57.3 3.0 %copy-start.1 = (bf16[1536,512]{1,0:T(8,128)(2,1)S(1)}, bf16[1536,512]{1,0:T(8,128)(2,1)}, u32[]{:S(2)}) copy-start(bf16[1536,512]{1,0:T(8,128)(2,1)} %get-tuple-element.38) | copy-start | bytes 4718596 | tf_op jit(solution)/shard_map/cond
  57.3 3.0 copy-start.13
  60.2 2.4 copy-start.11
  67.0 1.4 copy-start.2
  67.0 1.4 copy-start.6
  70.7 2.4 copy-start.7
  73.7 1.1 copy-start.14
  78.4 1.6 copy-start.9
  78.4 23.5 %copy-start.4 = (bf16[48,2048]{1,0:T(8,128)(2,1)S(1)}, bf16[48,2048]{1,0:T(8,128)(2,1)}, u32[]{:S(2)}) copy-start(bf16[48,2048]{1,0:T(8,128)(2,1)} %param.22) | copy-start | bytes 589828
  78.4 24.6 %copy-start.8 = (f32[2048]{0:T(1024)S(1)}, f32[2048]{0:T(1024)}, u32[]{:S(2)}) copy-start(f32[2048]{0:T(1024)} %param.33) | copy-start | bytes 24580
  113.1 61.2 %copy-start.12 = (bf16[1,2048,512]{2,1,0:T(8,128)(2,1)S(1)}, bf16[1,2048,512]{2,1,0:T(8,128)(2,1)}, u32[]{:S(2)}) copy-start(bf16[1,2048,512]{2,1,0:T(8,128)(2,1)} %param.39) | copy-start | bytes 6291460
  172.9 1.4 copy-start.3
  184.1 5.0 %copy-start.10 = (f32[192,2]{0,1:T(2,128)S(1)}, f32[192,2]{0,1:T(2,128)}, u32[]{:S(2)}) copy-start(f32[192,2]{0,1:T(2,128)} %param.35) | copy-start | bytes 4612
  184.1 58.0 %all-to-all-start.1 = ((bf16[8,72,2048]{2,1,0:T(8,128)(2,1)}), bf16[8,72,2048]{2,1,0:T(8,128)(2,1)}, u32[]{:S(2)}, u32[]{:S(2)}) async-start(bf16[8,72,2048]{2,1,0:T(8,128)(2,1)} %bitcast.97), calls=%async_computation.2 | async-start | bytes 4718592 | tf_op jit(solution)/shard_map/all_to_all | solution.py:201
  188.6 100.0 %reduce-scatter.5.cloned.1.call-start = ((), (), s32[]{:S(2)}) async-start(), calls=%async_computation.6 | async-start | bytes 983040 | tf_op jit(solution)/shard_map/reduce_scatter | solution.py:207
  261.7 26.9 %copy-start.5 = (bf16[48,2048]{1,0:T(8,128)(2,1)S(1)}, bf16[48,2048]{1,0:T(8,128)(2,1)}, u32[]{:S(2)}) copy-start(bf16[48,2048]{1,0:T(8,128)(2,1)} %reduce-scatter.3.cloned.1.call-done) | copy-start | bytes 589828
Sparse Core Ops, SparseCore 0:
  9.5 46.9 all-gather.2
  80.1 21.7 reduce-scatter.2
  266.7 21.8 reduce-scatter.4
where the time goes:
time: 297 us
  waiting for transfers between devices  106 us (36%)
  blocking collectives  101 us (34%)
  matrix products  37.6 us (13%)
  local copies, waits for them, and re-layouts  17.4 us (6%)
  other arithmetic  17.3 us (6%)
  between operations  13.3 us (4%)
  starting transfers between devices  4.59 us (2%)
    all_to_all x1, blocking collectives, shards(): lax.all_to_all(outgoing, 'sp', split_axis=0, concat_axis=0, tiled=True)  59.7 us
    all_to_all x1, waiting for transfers between devices, shards(): lax.all_to_all(part.reshape(sources, items, down_w.shape[1]), 'sp', split...  49.9 us
    all_gather x1, blocking collectives, shards(): rot_piece = lax.all_gather(rot_key, 'sp', axis=0, tiled=True)  32.5 us
    reduce_scatter x1, waiting for transfers between devices, shards(): lax.psum_scatter((term + jnp.sum(picked * route_weights[..., None], axis=...  22 us
    reduce_scatter x1, waiting for transfers between devices, shards(): lax.psum_scatter((term + jnp.einsum('hqv,hvd->qd', heads_out_b, proj_b, p...  19.8 us
    all_gather x1, waiting for transfers between devices, shards(): lat_rows = lax.all_gather(latents, 'sp', axis=0, tiled=True)  13.4 us
    gather x2, local copies, waits for them, and re-layouts, shards(): picked = jnp.take(back_flat, slots, axis=0).astype(jnp.float32)  10.8 us
    reduce_sum x1, other arithmetic, shards(): jnp.sum(picked * route_weights[..., None], axis=1)  8.74 us
  transfers between devices with their start and end apart: 4, of which 4 were waited for; matrix products, arithmetic and copies ran while one was open for 3% of the time, Pallas kernels for 0%

commit v1 on v0

--- a/solution.py
+++ b/solution.py
@@ -1,6 +1,10 @@
+import functools
+
 import jax
 import jax.numpy as jnp
 from jax import lax
+from jax.experimental import pallas as pl
+from jax.experimental.pallas import tpu as pltpu
 from jax.sharding import PartitionSpec as P
 
 DA = 64
@@ -13,6 +17,500 @@
 theta_base = 10000.0
 norm_eps = 1e-06
 very_low = -1e30
+kernel_vmem = 20 * 2**20
+
+MESH_ID = pl.DeviceIdType.MESH
+VMEM_SPEC = pl.BlockSpec(memory_space=pltpu.VMEM)
+
+
+def remote(src, dst, send, recv, device):
+    return pltpu.make_async_remote_copy(
+        src_ref=src, dst_ref=dst, send_sem=send, recv_sem=recv, device_id=device,
+        device_id_type=MESH_ID,
+    )
+
+
+def greet(devices):
+    barrier = pltpu.get_barrier_semaphore()
+    for device in devices:
+        pl.semaphore_signal(barrier, inc=1, device_id=device, device_id_type=MESH_ID)
+    pl.semaphore_wait(barrier, len(devices))
+
+
+def place_in_tp():
+    me = lax.axis_index("tp")
+    core = lax.rem(me, 2)
+    return me, core, me // 2, {"tp": me + 1 - 2 * core}
+
+
+def block_of(chips, chip, core):
+    return core * chips + chip
+
+
+def all_peers(n, chips):
+    me = lax.axis_index("sp")
+    near, mate = tp_chip_peers(chips)
+    return [{"sp": lax.rem(me + k, n)} for k in range(1, n)], near + [mate]
+
+
+def spread(chips, count, arrive, slot, ysend, yrecv, msend, mrecv):
+    _, core, chip, mate = place_in_tp()
+    near, far = [], []
+
+    def relay(item):
+        for i, j, copy in far:
+            if i == item:
+                copy.wait_recv()
+                block = slot(i, block_of(chips, lax.rem(chip + chips - j, chips), core))
+                onward = remote(block, block, msend.at[j, i], mrecv.at[j, i], mate)
+                onward.start()
+                near.append(onward)
+
+    for i in range(count):
+        arrive(i)
+        own = slot(i, block_of(chips, chip, core))
+        for j in range(1, chips):
+            copy = remote(
+                own, own, ysend.at[j - 1, i], yrecv.at[j - 1, i],
+                {"tp": 2 * lax.rem(chip + j, chips) + core},
+            )
+            copy.start()
+            far.append((i, j, copy))
+        copy = remote(own, own, msend.at[0, i], mrecv.at[0, i], mate)
+        copy.start()
+        near.append(copy)
+        if i:
+            relay(i - 1)
+    relay(count - 1)
+    for _, _, copy in far:
+        copy.wait_send()
+    for copy in near:
+        copy.wait()
+
+
+def spread_sems(chips, count):
+    return [pltpu.SemaphoreType.DMA((chips - 1, count))] * 2 + [
+        pltpu.SemaphoreType.DMA((chips, count))
+    ] * 2
+
+
+def gather_kernel(n, lat_ref, rot_ref, lat_out, rot_out, send, recv, fsend, frecv, local):
+    me = lax.axis_index("sp")
+    _, core, _, mate = place_in_tp()
+    pairs = ((lat_ref, lat_out), (rot_ref, rot_out))
+    own = [
+        pltpu.make_async_copy(src, dst.at[me], local.at[a]) for a, (src, dst) in enumerate(pairs)
+    ]
+    for copy in own:
+        copy.start()
+    peers = [{"sp": lax.rem(me + k, n)} for k in range(1, n)]
+    greet(peers + [mate])
+    copies = []
+    for k in range(1, n):
+        for a, (src, dst) in enumerate(pairs):
+            copy = remote(
+                src.at[core], dst.at[me, core], send.at[a, k - 1], recv.at[a, k - 1], peers[k - 1]
+            )
+            copy.start()
+            copies.append(copy)
+    forwards = []
+    for k in range(1, n):
+        origin = lax.rem(me + n - k, n)
+        for a, (src, dst) in enumerate(pairs):
+            copies[2 * (k - 1) + a].wait_recv()
+            forward = remote(
+                dst.at[origin, core], dst.at[origin, core], fsend.at[a, k - 1],
+                frecv.at[a, k - 1], mate,
+            )
+            forward.start()
+            forwards.append(forward)
+    for copy in own:
+        copy.wait()
+    for copy in copies:
+        copy.wait_send()
+    for forward in forwards:
+        forward.wait()
+
+
+def gather_latents(latents, rot_key):
+    n = lax.axis_size("sp")
+    tok, rank = latents.shape
+    rope = rot_key.shape[1]
+    half = tok // 2
+    lat, rot = pl.pallas_call(
+        functools.partial(gather_kernel, n),
+        out_shape=(
+            jax.ShapeDtypeStruct((n, 2, half, rank), latents.dtype),
+            jax.ShapeDtypeStruct((n, 2, half * rope // 128, 128), rot_key.dtype),
+        ),
+        in_specs=[VMEM_SPEC] * 2,
+        out_specs=(VMEM_SPEC,) * 2,
+        scratch_shapes=[pltpu.SemaphoreType.DMA((2, n - 1))] * 4 + [pltpu.SemaphoreType.DMA((2,))],
+        compiler_params=pltpu.CompilerParams(collective_id=0, has_side_effects=True, vmem_limit_bytes=kernel_vmem),
+        name="gather_latents",
+    )(latents.reshape(2, half, rank), rot_key.reshape(2, half * rope // 128, 128))
+    return lat.reshape(n * tok, rank), rot.reshape(n * tok, rope)
+
+
+def scatter_sum(chips, term_ref, base_ref, from_mate, pair, landed, sems):
+    psend, precv, csend, crecv = sems
+    me, core, chip, mate = place_in_tp()
+    first = []
+    for k in list(range(1, chips)) + [0]:
+        where = lax.rem(chip + k, chips)
+        copy = remote(
+            term_ref.at[2 * where + 1 - core], from_mate.at[k], psend.at[k], precv.at[k], mate
+        )
+        copy.start()
+        first.append((k, where, copy))
+    second = []
+    for k, where, copy in first:
+        copy.wait_recv()
+        total = term_ref[2 * where + core].astype(jnp.float32) + from_mate[k].astype(jnp.float32)
+        if k:
+            pair[k - 1] = total.astype(jnp.bfloat16)
+            out = remote(
+                pair.at[k - 1], landed.at[k - 1], csend.at[k - 1], crecv.at[k - 1],
+                {"tp": 2 * where + core},
+            )
+            out.start()
+            second.append(out)
+    for k, out in enumerate(second):
+        out.wait_recv()
+        total = total + landed[k].astype(jnp.float32)
+    for _, _, copy in first:
+        copy.wait_send()
+    for out in second:
+        out.wait_send()
+    return base_ref[...].astype(jnp.float32) + total
+
+
+def tp_chip_peers(chips):
+    _, core, chip, mate = place_in_tp()
+    return [{"tp": 2 * lax.rem(chip + k, chips) + core} for k in range(1, chips)], mate
+
+
+def norm_kernel(
+    chips, term_ref, base_ref, gain_ref, hidden_ref, rows_ref,
+    from_mate, pair, landed, psend, precv, csend, crecv, asend, arecv, fsend, frecv,
+):
+    me, core, chip, mate = place_in_tp()
+    peers, _ = tp_chip_peers(chips)
+    greet(peers + [mate])
+    state = scatter_sum(
+        chips, term_ref, base_ref, from_mate, pair, landed, (psend, precv, csend, crecv)
+    ).astype(jnp.bfloat16)
+    hidden_ref[...] = state
+    wide = state.astype(jnp.float32)
+    normed = wide * lax.rsqrt(jnp.mean(wide * wide, axis=-1, keepdims=True) + norm_eps)
+    rows_ref[me] = (normed * gain_ref[...]).astype(jnp.bfloat16)
+    copies = []
+    for k in range(1, chips):
+        copy = remote(rows_ref.at[me], rows_ref.at[me], asend.at[k], arecv.at[k], peers[k - 1])
+        copy.start()
+        copies.append(copy)
+    near = remote(rows_ref.at[me], rows_ref.at[me], asend.at[0], arecv.at[0], mate)
+    near.start()
+    forwards = []
+    for k in range(1, chips):
+        copies[k - 1].wait_recv()
+        origin = 2 * lax.rem(chip + chips - k, chips) + core
+        forward = remote(
+            rows_ref.at[origin], rows_ref.at[origin], fsend.at[k - 1], frecv.at[k - 1], mate
+        )
+        forward.start()
+        forwards.append(forward)
+    near.wait()
+    for copy in copies:
+        copy.wait_send()
+    for forward in forwards:
+        forward.wait()
+
+
+def final_kernel(
+    chips, term_ref, base_ref, out_ref, from_mate, pair, landed, psend, precv, csend, crecv
+):
+    peers, mate = tp_chip_peers(chips)
+    greet(peers + [mate])
+    out_ref[...] = scatter_sum(
+        chips, term_ref, base_ref, from_mate, pair, landed, (psend, precv, csend, crecv)
+    ).astype(jnp.bfloat16)
+
+
+def sum_scratch(chips, rows, width):
+    return [
+        pltpu.VMEM((chips, rows, width), jnp.bfloat16),
+        pltpu.VMEM((chips - 1, rows, width), jnp.bfloat16),
+        pltpu.VMEM((chips - 1, rows, width), jnp.bfloat16),
+        pltpu.SemaphoreType.DMA((chips,)),
+        pltpu.SemaphoreType.DMA((chips,)),
+        pltpu.SemaphoreType.DMA((chips - 1,)),
+        pltpu.SemaphoreType.DMA((chips - 1,)),
+    ]
+
+
+def mix_and_norm(term, residual, gain):
+    devices = lax.axis_size("tp")
+    chips = devices // 2
+    rows, width = residual.shape
+    hidden, whole = pl.pallas_call(
+        functools.partial(norm_kernel, chips),
+        out_shape=(
+            jax.ShapeDtypeStruct((rows, width), jnp.bfloat16),
+            jax.ShapeDtypeStruct((devices, rows, width), jnp.bfloat16),
+        ),
+        in_specs=[VMEM_SPEC] * 3,
+        out_specs=(VMEM_SPEC,) * 2,
+        scratch_shapes=sum_scratch(chips, rows, width)
+        + [pltpu.SemaphoreType.DMA((chips,))] * 2
+        + [pltpu.SemaphoreType.DMA((chips - 1,))] * 2,
+        compiler_params=pltpu.CompilerParams(collective_id=1, has_side_effects=True, vmem_limit_bytes=kernel_vmem),
+        name="mix_and_norm",
+    )(term.reshape(devices, rows, width), residual, gain.reshape(1, width))
+    return hidden, whole.reshape(devices * rows, width)
+
+
+def final_sum(term, hidden):
+    devices = lax.axis_size("tp")
+    chips = devices // 2
+    rows, width = hidden.shape
+    return pl.pallas_call(
+        functools.partial(final_kernel, chips),
+        out_shape=jax.ShapeDtypeStruct((rows, width), jnp.bfloat16),
+        in_specs=[VMEM_SPEC] * 2,
+        out_specs=VMEM_SPEC,
+        scratch_shapes=sum_scratch(chips, rows, width),
+        compiler_params=pltpu.CompilerParams(collective_id=4, has_side_effects=True, vmem_limit_bytes=kernel_vmem),
+        name="final_sum",
+    )(term.reshape(devices, rows, width), hidden)
+
+
+def dispatch_kernel(n, chips, out_ref, got_ref, send, recv, local, *sems):
+    me = lax.axis_index("sp")
+    _, core, chip, _ = place_in_tp()
+    mine = block_of(chips, chip, core)
+    cols = out_ref.shape[2]
+
+    def slot(source, block):
+        return got_ref.at[source, :, pl.ds(pl.multiple_of(block * cols, cols), cols)]
+
+    own = pltpu.make_async_copy(out_ref.at[me], slot(me, mine), local.at[0])
+    own.start()
+    peers, group = all_peers(n, chips)
+    greet(peers + group)
+    copies = []
+    for k in range(1, n):
+        copy = remote(
+            out_ref.at[lax.rem(me + k, n)], slot(me, mine), send.at[k], recv.at[k], peers[k - 1]
+        )
+        copy.start()
+        copies.append(copy)
+    spread(
+        chips,
+        n,
+        lambda i: copies[i - 1].wait_recv() if i else own.wait(),
+        lambda i, block: slot(lax.rem(me + n - i, n), block),
+        *sems,
+    )
+    for copy in copies:
+        copy.wait_send()
+
+
+def dispatch(outgoing):
+    n, items, cols = outgoing.shape
+    devices = lax.axis_size("tp")
+    return pl.pallas_call(
+        functools.partial(dispatch_kernel, n, devices // 2),
+        out_shape=jax.ShapeDtypeStruct((n, items, cols * devices), jnp.bfloat16),
+        in_specs=[VMEM_SPEC],
+        out_specs=VMEM_SPEC,
+        scratch_shapes=[pltpu.SemaphoreType.DMA((n,))] * 2
+        + [pltpu.SemaphoreType.DMA((1,))]
+        + spread_sems(devices // 2, n),
+        compiler_params=pltpu.CompilerParams(collective_id=2, has_side_effects=True, vmem_limit_bytes=kernel_vmem),
+        name="dispatch",
+    )(outgoing)
+
+
+def return_kernel(
+    n, chips, part_ref, back_ref, from_mate, pair, landed, ready,
+    psend, precv, ysend, yrecv, send, recv,
+):
+    me = lax.axis_index("sp")
+    _, core, chip, mate = place_in_tp()
+    cols = back_ref.shape[2]
+    half = cols * chips
+    peers, group = all_peers(n, chips)
+    greet(peers + group)
+
+    def columns(start, width):
+        return pl.ds(pl.multiple_of(start * width, width), width)
+
+    order = list(range(1, n)) + [0]
+    first, second, third = [], [], []
+    for k in order:
+        copy = remote(
+            part_ref.at[lax.rem(me + k, n), :, columns(1 - core, half)], from_mate.at[k],
+            psend.at[k], precv.at[k], mate,
+        )
+        copy.start()
+        first.append(copy)
+    for k, copy in zip(order, first):
+        copy.wait_recv()
+        total = part_ref[lax.rem(me + k, n), :, columns(core, half)].astype(jnp.float32)
+        pair[k] = (total + from_mate[k].astype(jnp.float32)).astype(jnp.bfloat16)
+        for j in range(1, chips):
+            where = lax.rem(chip + j, chips)
+            out = remote(
+                pair.at[k, :, columns(where, cols)], landed.at[j - 1, k],
+                ysend.at[j - 1, k], yrecv.at[j - 1, k], {"tp": 2 * where + core},
+            )
+            out.start()
+            second.append((k, j, out))
+    for k in order:
+        total = pair[k, :, columns(chip, cols)].astype(jnp.float32)
+        for i, j, out in second:
+            if i == k:
+                out.wait_recv()
+                total = total + landed[j - 1, k].astype(jnp.float32)
+        if k:
+            ready[k - 1] = total.astype(jnp.bfloat16)
+            home = remote(
+                ready.at[k - 1], back_ref.at[me], send.at[k - 1], recv.at[k - 1], peers[k - 1]
+            )
+            home.start()
+            third.append(home)
+        else:
+            back_ref[me] = total.astype(jnp.bfloat16)
+    for copy in first:
+        copy.wait_send()
+    for _, _, out in second:
+        out.wait_send()
+    for home in third:
+        home.wait()
+
+
+def return_parts(part):
+    n, items, width = part.shape
+    devices = lax.axis_size("tp")
+    chips = devices // 2
+    cols = width // devices
+    return pl.pallas_call(
+        functools.partial(return_kernel, n, chips),
+        out_shape=jax.ShapeDtypeStruct((n, items, cols), jnp.bfloat16),
+        in_specs=[VMEM_SPEC],
+        out_specs=VMEM_SPEC,
+        scratch_shapes=[
+            pltpu.VMEM((n, items, width // 2), jnp.bfloat16),
+            pltpu.VMEM((n, items, width // 2), jnp.bfloat16),
+            pltpu.VMEM((chips - 1, n, items, cols), jnp.bfloat16),
+            pltpu.VMEM((n - 1, items, cols), jnp.bfloat16),
+            pltpu.SemaphoreType.DMA((n,)),
+            pltpu.SemaphoreType.DMA((n,)),
+            pltpu.SemaphoreType.DMA((chips - 1, n)),
+            pltpu.SemaphoreType.DMA((chips - 1, n)),
+            pltpu.SemaphoreType.DMA((n - 1,)),
+            pltpu.SemaphoreType.DMA((n - 1,)),
+        ],
+        compiler_params=pltpu.CompilerParams(collective_id=3, has_side_effects=True, vmem_limit_bytes=kernel_vmem),
+        name="return_parts",
+    )(part)
+
+
+def whole_block(shape):
+    return pl.BlockSpec(shape, lambda i: (0,) * len(shape))
+
+
+def column_block(shape, cols):
+    return pl.BlockSpec((shape[0], cols), lambda i: (0, i))
+
+
+def column_call(body, name, whole, tiled, rows, cols, dtype, flops):
+    width = tiled[0].shape[1]
+    moved = sum(a.size * a.dtype.itemsize for a in (*whole, *tiled)) + rows * width * 2
+    return pl.pallas_call(
+        body,
+        out_shape=jax.ShapeDtypeStruct((rows, width), dtype),
+        grid=(width // cols,),
+        in_specs=[whole_block(a.shape) for a in whole]
+        + [column_block(a.shape, cols) for a in tiled],
+        out_specs=column_block((rows, width), cols),
+        cost_estimate=pl.CostEstimate(flops=flops, bytes_accessed=moved, transcendentals=0),
+        compiler_params=pltpu.CompilerParams(dimension_semantics=("arbitrary",), vmem_limit_bytes=kernel_vmem),
+        name=name,
+    )(*whole, *tiled)
+
+
+def dot32(a, b):
+    return jnp.dot(a, b, preferred_element_type=jnp.float32)
+
+
+def tile_of(width, most):
+    cols = min(width, most)
+    return cols if width % cols == 0 else 128
+
+
+def gated_body(rows_ref, gate_ref, up_ref, out_ref):
+    gate = dot32(rows_ref[...], gate_ref[...])
+    up = dot32(rows_ref[...], up_ref[...])
+    out_ref[...] = (gate / (1.0 + jnp.exp(-gate)) * up).astype(jnp.bfloat16)
+
+
+def gated(rows, gate, up, name):
+    count, width = rows.shape
+    hidden = gate.shape[1]
+    return column_call(
+        gated_body, name, (rows,), (gate, up), count, tile_of(hidden, 256), jnp.bfloat16,
+        4 * count * width * hidden,
+    )
+
+
+def product_body(rows_ref, weight_ref, out_ref):
+    out_ref[...] = dot32(rows_ref[...], weight_ref[...]).astype(jnp.bfloat16)
+
+
+def product(rows, weight, name):
+    return column_call(
+        product_body, name, (rows,), (weight,), rows.shape[0], tile_of(weight.shape[1], 512),
+        jnp.bfloat16, 2 * rows.shape[0] * weight.size,
+    )
+
+
+def project_body(a_ref, b_ref, pa_ref, pb_ref, out_ref):
+    total = jnp.zeros(out_ref.shape, jnp.float32)
+    for heads_ref, weight_ref in ((a_ref, pa_ref), (b_ref, pb_ref)):
+        size = heads_ref.shape[2]
+        for h in range(heads_ref.shape[0]):
+            total += dot32(heads_ref[h], weight_ref[h * size : (h + 1) * size, :])
+    out_ref[...] = total.astype(jnp.bfloat16)
+
+
+def project(heads_a, heads_b, proj_a, proj_b):
+    rows = heads_a.shape[1]
+    return column_call(
+        project_body, "project", (heads_a, heads_b), (proj_a, proj_b), rows,
+        tile_of(proj_a.shape[1], 512), jnp.bfloat16, 2 * rows * (proj_a.size + proj_b.size),
+    )
+
+
+def combine_body(act_ref, back_ref, slots_ref, weights_ref, down_ref, out_ref):
+    _, core, chip, _ = place_in_tp()
+    block = block_of(lax.axis_size("tp") // 2, chip, core)
+    term = dot32(act_ref[...], down_ref[...])
+    here = pl.program_id(0) == block
+
+    @pl.when(here)
+    def _():
+        total = term
+        spots = lax.broadcasted_iota(jnp.int32, (act_ref.shape[0], back_ref.shape[0]), 1)
+        for k in range(slots_ref.shape[1]):
+            chosen = (spots == slots_ref[:, k : k + 1]).astype(jnp.float32).astype(jnp.bfloat16)
+            total += dot32(chosen, back_ref[...]) * weights_ref[:, k : k + 1]
+        out_ref[...] = total.astype(jnp.bfloat16)
+
+    @pl.when(jnp.logical_not(here))
+    def _():
+        out_ref[...] = term.astype(jnp.bfloat16)
 
 
 def tables(positions, width):
@@ -82,7 +580,6 @@
     heads_a = key_up_a.shape[1] // DA
     heads_b = key_up_b.shape[1] // DB
     first_row = lax.axis_index("sp") * tok
-    last_row = first_row + tok
     query_pos = first_row + jnp.arange(tok, dtype=jnp.int32)
     cosine, sine = tables(query_pos, ROPE)
     rot_key = rotate(rope_key, cosine, sine)
@@ -136,39 +633,19 @@
         return (keys_a, values_a, keys_b, values_b)
 
     start_state = (empty_state(heads_a, tok, VA), empty_state(heads_b, tok, VB))
-    lat_rows = lax.all_gather(latents, "sp", axis=0, tiled=True)
-    rot_piece = lax.all_gather(rot_key, "sp", axis=0, tiled=True)
+    lat_rows, rot_piece = gather_latents(latents, rot_key)
     key_pos = jnp.arange(lat_rows.shape[0], dtype=jnp.int32)
 
     def compute(inner):
         keys_a, values_a, keys_b, values_b = project_latents(lat_rows)
         return attend(inner, keys_a, values_a, keys_b, values_b, rot_piece, key_pos)
 
-    state = lax.cond(jnp.int32(0) < last_row, compute, lambda inner: inner, start_state)
+    state = compute(start_state)
     heads_out_a = (state[0][2] / state[0][1][..., None]).astype(jnp.bfloat16)
     heads_out_b = (state[1][2] / state[1][1][..., None]).astype(jnp.bfloat16)
-    proj_a = out_proj_a.reshape(heads_a, VA, out_proj_a.shape[1])
-    proj_b = out_proj_b.reshape(heads_b, VB, out_proj_b.shape[1])
-    term = jnp.einsum("hqv,hvd->qd", heads_out_a, proj_a, preferred_element_type=jnp.float32)
-    mixed = lax.psum_scatter(
-        (
-            term
-            + jnp.einsum("hqv,hvd->qd", heads_out_b, proj_b, preferred_element_type=jnp.float32)
-        ).astype(jnp.bfloat16),
-        "tp",
-        scatter_dimension=0,
-        tiled=True,
-    ).astype(jnp.float32)
-    hidden_state = (residual.astype(jnp.float32) + mixed).astype(jnp.bfloat16)
-    wide = hidden_state.astype(jnp.float32)
-    normed = (
-        wide * lax.rsqrt(jnp.mean(wide * wide, axis=-1, keepdims=True) + norm_eps) * norm_gain
-    ).astype(jnp.bfloat16)
-    whole_rows = lax.all_gather(normed, "tp", axis=0, tiled=True)
-    shared_act = (
-        jax.nn.silu(jnp.dot(whole_rows, shared_gate, preferred_element_type=jnp.float32))
-        * jnp.dot(whole_rows, shared_up, preferred_element_type=jnp.float32)
-    ).astype(jnp.bfloat16)
+    term = project(heads_out_a, heads_out_b, out_proj_a, out_proj_b)
+    hidden_state, whole_rows = mix_and_norm(term, residual, norm_gain)
+    shared_act = gated(whole_rows, shared_gate, shared_up, "shared_act")
     experts = lax.axis_size("sp")
     topk = routes.shape[1]
     capacity = max(2, 3 * tok * topk // (2 * experts))
@@ -177,40 +654,33 @@
     before = jnp.cumsum(onehot, axis=0) - onehot
     rank = jnp.sum(before * onehot, axis=1)
     slots = (flat * capacity + rank).reshape(tok, topk)
-    placing = jnp.sum(
-        (
-            slots[:, :, None] == jnp.arange(experts * capacity, dtype=jnp.int32)[None, None, :]
-        ).astype(jnp.bfloat16),
-        axis=1,
-    )
+    spots = jnp.arange(experts * capacity, dtype=jnp.int32)
+    chosen = (slots[:, :, None] == spots[None, None, :]).astype(jnp.bfloat16)
+    devices = lax.axis_size("tp")
+    me = lax.axis_index("tp")
+    width = whole_rows.shape[1]
+    cols = width // devices
+    start = block_of(devices // 2, me // 2, lax.rem(me, 2)) * cols
     outgoing = jnp.einsum(
-        "rs,rd->sd", placing, whole_rows, preferred_element_type=jnp.float32
+        "rs,rd->sd",
+        jnp.sum(chosen, axis=1),
+        lax.dynamic_slice_in_dim(whole_rows, start, cols, axis=1),
+        preferred_element_type=jnp.float32,
     ).astype(jnp.bfloat16)
-    outgoing = outgoing.reshape(experts, capacity, whole_rows.shape[1])
     gate_w = expert_gate[0]
     up_w = expert_up[0]
     down_w = expert_down[0]
-    arrived = lax.all_to_all(outgoing, "sp", split_axis=0, concat_axis=0, tiled=True)
-    sources, items, width = arrived.shape
-    rows_in = arrived.reshape(sources * items, width)
-    act = (
-        jax.nn.silu(jnp.dot(rows_in, gate_w, preferred_element_type=jnp.float32))
-        * jnp.dot(rows_in, up_w, preferred_element_type=jnp.float32)
-    ).astype(jnp.bfloat16)
-    part = jnp.dot(act, down_w, preferred_element_type=jnp.float32).astype(jnp.bfloat16)
-    back = lax.all_to_all(
-        part.reshape(sources, items, down_w.shape[1]), "sp", split_axis=0, concat_axis=0, tiled=True
-    )
-    back_flat = back.reshape(experts * capacity, back.shape[2])
-    term = jnp.dot(shared_act, shared_down, preferred_element_type=jnp.float32)
-    picked = jnp.take(back_flat, slots, axis=0).astype(jnp.float32)
-    moe = lax.psum_scatter(
-        (term + jnp.sum(picked * route_weights[..., None], axis=1)).astype(jnp.bfloat16),
-        "tp",
-        scatter_dimension=0,
-        tiled=True,
-    ).astype(jnp.float32)
-    return (hidden_state.astype(jnp.float32) + moe).astype(jnp.bfloat16)
+    arrived = dispatch(outgoing.reshape(experts, capacity, cols))
+    rows_in = arrived.reshape(experts * capacity, width)
+    act = gated(rows_in, gate_w, up_w, "expert_act")
+    part = product(act, down_w, "expert_part")
+    back = return_parts(part.reshape(experts, capacity, width))
+    back_flat = back.reshape(experts * capacity, cols)
+    term = column_call(
+        combine_body, "combine", (shared_act, back_flat, slots, route_weights), (shared_down,), tok,
+        cols, jnp.bfloat16, 2 * tok * shared_down.size,
+    )
+    return final_sum(term, hidden_state)
 
 
 def solution(mesh):

time: 297 us -> 141 us (0.47)
  Pallas kernels: 0 us -> 113 us
  waiting for transfers between devices: 106 us -> 0 us
  blocking collectives: 101 us -> 0 us
  matrix products: 37.6 us -> 10.4 us
  between operations: 13.3 us -> 0.47 us
  other arithmetic: 17.3 us -> 4.92 us
  local copies, waits for them, and re-layouts: 17.4 us -> 11.6 us
  starting transfers between devices: 4.59 us -> 0 us
    pallas_call x0 -> x10, Pallas kernels: none -> 113 us  [the longest x1 31.1 us: dispatch(): pl.pallas_call(functools.partial(dispatch_kernel, n, devices // 2), out_s...]
    all_to_all x1 -> x0, blocking collectives: 59.7 us -> none  [shards(): lax.all_to_all(outgoing, 'sp', split_axis=0, concat_axis=0, tiled=True)]
    all_to_all x1 -> x0, waiting for transfers between devices: 49.9 us -> none  [shards(): lax.all_to_all(part.reshape(sources, items, down_w.shape[1]), 'sp', split...]
    reduce_scatter x2 -> x0, waiting for transfers between devices: 41.9 us -> none  [the longest x1 22 us: shards(): lax.psum_scatter((term + jnp.sum(picked * route_weights[..., None], axis=...]
    all_gather x2 -> x0, blocking collectives: 40.8 us -> none  [the longest x1 32.5 us: shards(): rot_piece = lax.all_gather(rot_key, 'sp', axis=0, tiled=True)]
    dot_general x7 -> x1, matrix products: 21.6 us -> 0.34 us  [shards(): jnp.einsum('rs,rd->sd', jnp.sum(chosen, axis=1), lax.dynamic_slice_in_dim...]
    all_gather x1 -> x0, waiting for transfers between devices: 13.4 us -> none  [shards(): lat_rows = lax.all_gather(latents, 'sp', axis=0, tiled=True)]
    gather x2 -> x0, local copies, waits for them, and re-layouts: 10.8 us -> none  [shards(): picked = jnp.take(back_flat, slots, axis=0).astype(jnp.float32)]
  transfers between devices with their start and end apart: 4 -> 0, of which waited for: 4 -> 0; matrix products, arithmetic and copies ran while one was open for 3% -> 0% of each run, Pallas kernels for 0% -> 0%
where the time goes in v1:
time: 141 us
  Pallas kernels  113 us (80%)
  local copies, waits for them, and re-layouts  11.6 us (8%)
  matrix products  10.4 us (7%)
  other arithmetic  4.92 us (3%)
    pallas_call x1, Pallas kernels, dispatch(): pl.pallas_call(functools.partial(dispatch_kernel, n, devices // 2), out_s...  31.1 us
    pallas_call x1, Pallas kernels, return_parts(): pl.pallas_call(functools.partial(return_kernel, n, chips), out_shape=jax....  24.9 us
    pallas_call x1, Pallas kernels, gather_latents(): pl.pallas_call(functools.partial(gather_kernel, n), out_shape=(jax.ShapeD...  21 us
    pallas_call x1, Pallas kernels, mix_and_norm(): pl.pallas_call(functools.partial(norm_kernel, chips), out_shape=(jax.Shap...  16.4 us
    pallas_call x5, Pallas kernels, column_call(): pl.pallas_call(body, out_shape=jax.ShapeDtypeStruct((rows, width), dtype)...  11.4 us
    unnamed x49, local copies, waits for them, and re-layouts  10.3 us
    pallas_call x1, Pallas kernels, final_sum(): pl.pallas_call(functools.partial(final_kernel, chips), out_shape=jax.Shap...  8.46 us

profile of v1, /device:TPU:0, one launch (start us, length us, event | category | flops | bytes accessed | tf_op | source)
XLA Modules:
  0.0 140.6 jit_solution(7002480434458167171)
XLA Ops:
  0.0 0.9 multiply_cosine_fusion
  0.9 1.1 copy.66
  2.1 1.0 copy.63
  3.4 0.9 copy-done.12
  4.3 21.0 %gather_latents.1 = (bf16[8,2,96,512]{3,2,1,0:T(8,128)(2,1)S(1)}, bf16[8,2,24,128]{3,2,1,0:T(8,128)(2,1)S(1)}) custom-call(bf16[2,96,512]{2,1,0:T(8,128)(2,1)S(1)} %bitcast.80, bf16[2,24,128]{2,1,0:T(8,128)(2,1)S(1)} %convert_element_type.74.rot_ref), custom_call_target="tpu_custom_call" | custom-call | tf_op jit(solution)/shard_map/gather_latents/pallas_call | solution.py:140
  25.5 0.8 fusion.32
  26.3 1.0 convolution_convert_fusion.1
  27.6 1.6 %fusion.67 = (f32[4,192]{1,0:T(4,128)S(1)}, f32[4,192,1536]{2,1,0:T(8,128)S(1)}) fusion(f32[1536,192,4]{0,1,2:T(8,128)S(1)} %fusion.32, bf16[1536,4,128]{0,2,1:T(8,128)(2,1)S(1)} %bitcast.85, bf16[192,4,160]{0,2,1:T(8,128)(2,1)S(1)} %bitcast.87, pred[192,1536]{1,0:T(8,128)(4,1)S(1)} %iota_compare_fusion), kind=kOutput, calls=%fused_computation.92 | convolution fusion | flops 306707712 | bytes 11570176 | tf_op jit(solution)/shard_map/qhd,khd->hqk/dot_general | solution.py:535
  29.3 0.6 convolution_convert_fusion.3
  29.9 0.8 fusion.37
  30.7 1.5 %fusion.66 = (f32[4,192]{1,0:T(4,128)S(1)}, f32[4,192,1536]{2,1,0:T(8,128)S(1)}) fusion(bf16[192,4,16]{0,2,1:T(8,128)(2,1)S(1)} %get-tuple-element.19, bf16[192,4,16]{0,2,1:T(8,128)(2,1)S(1)} %get-tuple-element.20, bf16[1536,32]{1,0:T(8,128)(2,1)S(1)} %reshape.172, f32[4,1536,192]{1,2,0:T(8,128)S(1)} %fusion.37, pred[192,1536]{1,0:T(8,128)(4,1)S(1)} %iota_compare_fusion), kind=kOutput, calls=%fused_computation.91 | convolution fusion | flops 80313600 | bytes 9882624 | tf_op jit(solution)/shard_map/qhr,kr->hqk/dot_general | solution.py:536
  32.2 2.3 %fusion.6 = (f32[4,192]{1,0:T(4,128)S(1)}, f32[4,192]{1,0:T(4,128)S(1)}) fusion(f32[4,192,1536]{2,1,0:T(8,128)S(1)} %get-tuple-element.30, f32[4,192]{1,0:T(4,128)S(1)} %broadcast_maximum_fusion, pred[192,1536]{1,0:T(8,128)(4,1)S(1)} %iota_compare_fusion, f32[4,192,1536]{2,1,0:T(8,128)S(1)} %get-tuple-element.28, f32[4,192]{1,0:T(4,128)S(1)} %broadcast_maximum_fusion.1), kind=kLoop, calls=%fused_computation.10 | loop fusion | flops 7076352 | bytes 9744384 | tf_op jit(solution)/shard_map/reduce_sum | solution.py:542
  34.6 1.0 convolution_convert_fusion
  35.6 1.0 fusion.27.b_ref
  36.7 0.6 convolution_convert_fusion.2
  37.3 1.0 fusion.21.a_ref
  39.2 2.5 %project.1 = bf16[192,2048]{1,0:T(8,128)(2,1)S(1)} custom-call(bf16[4,192,64]{2,1,0:T(8,128)(2,1)S(1)} %fusion.21.a_ref, bf16[4,192,128]{2,1,0:T(8,128)(2,1)S(1)} %fusion.27.b_ref, bf16[256,2048]{1,0:T(8,128)(2,1)S(1)} %copy-done.8, bf16[512,2048]{1,0:T(8,128)(2,1)S(1)} %copy-done.1), custom_call_target="tpu_custom_call" | custom-call | flops 603979776 | bytes 4227072 | tf_op jit(solution)/shard_map/project/pallas_call | solution.py:431
  41.7 16.4 %mix_and_norm.1 = (bf16[48,2048]{1,0:T(8,128)(2,1)S(1)}, bf16[4,48,2048]{2,1,0:T(8,128)(2,1)S(1)}) custom-call(bf16[4,48,2048]{2,1,0:T(8,128)(2,1)S(1)} %bitcast.73, bf16[48,2048]{1,0:T(8,128)(2,1)S(1)} %copy-done.13, f32[1,2048]{1,0:T(1,128)S(1)} %bitcast.81), custom_call_target="tpu_custom_call" | custom-call | tf_op jit(solution)/shard_map/mix_and_norm/pallas_call | solution.py:256
  58.2 0.7 copy-done.10
  59.1 1.0 reduce-window.6
  61.6 31.1 %dispatch.1 = bf16[8,72,2048]{2,1,0:T(8,128)(2,1)S(1)} custom-call(bf16[8,72,512]{2,1,0:T(8,128)(2,1)S(1)} %bitcast.75), custom_call_target="tpu_custom_call" | custom-call | tf_op jit(solution)/shard_map/dispatch/pallas_call | solution.py:322
  92.7 1.6 %copy-done.15 = bf16[1,2048,512]{2,1,0:T(8,128)(2,1)S(1)} copy-done((bf16[1,2048,512]{2,1,0:T(8,128)(2,1)S(1)}, bf16[1,2048,512]{2,1,0:T(8,128)(2,1)}, u32[]{:S(2)}) %copy-start.15) | copy-done | bytes 2097176
  94.3 1.6 %copy-done.16 = bf16[1,2048,512]{2,1,0:T(8,128)(2,1)S(1)} copy-done((bf16[1,2048,512]{2,1,0:T(8,128)(2,1)S(1)}, bf16[1,2048,512]{2,1,0:T(8,128)(2,1)}, u32[]{:S(2)}) %copy-start.16) | copy-done | bytes 2097176
  95.9 3.1 %expert_act.1.rows_ref = bf16[576,512]{1,0:T(8,128)(2,1)S(1)} custom-call(bf16[576,2048]{1,0:T(8,128)(2,1)S(1)} %bitcast.74, bf16[2048,512]{1,0:T(8,128)(2,1)S(1)} %bitcast.82, bf16[2048,512]{1,0:T(8,128)(2,1)S(1)} %bitcast.83), custom_call_target="tpu_custom_call" | custom-call | flops 2415919104 | bytes 7143424 | tf_op jit(solution)/shard_map/expert_act/pallas_call | solution.py:431
  99.1 2.2 %expert_part.1 = bf16[576,2048]{1,0:T(8,128)(2,1)S(1)} custom-call(bf16[576,512]{1,0:T(8,128)(2,1)S(1)} %expert_act.1.rows_ref, bf16[512,2048]{1,0:T(8,128)(2,1)S(1)} %bitcast.77), custom_call_target="tpu_custom_call" | custom-call | flops 1207959552 | bytes 5046272 | tf_op jit(solution)/shard_map/expert_part/pallas_call | solution.py:431
  101.3 24.9 %return_parts.1 = bf16[8,72,512]{2,1,0:T(8,128)(2,1)S(1)} custom-call(bf16[8,72,2048]{2,1,0:T(8,128)(2,1)S(1)} %bitcast.67), custom_call_target="tpu_custom_call" | custom-call | tf_op jit(solution)/shard_map/return_parts/pallas_call | solution.py:398
  126.3 1.6 %shared_act.1.act_ref = bf16[192,512]{1,0:T(8,128)(2,1)S(1)} custom-call(bf16[192,2048]{1,0:T(8,128)(2,1)S(1)} %bitcast.79, bf16[2048,512]{1,0:T(8,128)(2,1)S(1)} %copy-done.3, bf16[2048,512]{1,0:T(8,128)(2,1)S(1)} %copy-done.4), custom_call_target="tpu_custom_call" | custom-call | flops 805306368 | bytes 5177344 | tf_op jit(solution)/shard_map/shared_act/pallas_call | solution.py:431
  127.8 0.8 copy.75.weights_ref
  128.6 0.9 copy-done.9
  129.5 2.0 %combine.1 = bf16[192,2048]{1,0:T(8,128)(2,1)S(1)} custom-call(bf16[192,512]{1,0:T(8,128)(2,1)S(1)} %shared_act.1.act_ref, bf16[576,512]{1,0:T(8,128)(2,1)S(1)} %bitcast.76, s32[192,2]{1,0:T(8,128)S(1)} %add.48.slots_ref, f32[192,2]{1,0:T(8,128)S(1)} %copy-done.9, bf16[512,2048]{1,0:T(8,128)(2,1)S(1)} %copy-done.5), custom_call_target="tpu_custom_call" | custom-call | flops 402653184 | bytes 3673088 | tf_op jit(solution)/shard_map/combine/pallas_call | solution.py:431
  131.5 8.5 %final_sum.1 = bf16[48,2048]{1,0:T(8,128)(2,1)S(1)} custom-call(bf16[4,48,2048]{2,1,0:T(8,128)(2,1)S(1)} %bitcast.72, bf16[48,2048]{1,0:T(8,128)(2,1)S(1)} %copy-done.11), custom_call_target="tpu_custom_call" | custom-call | tf_op jit(solution)/shard_map/final_sum/pallas_call | solution.py:277
  139.9 0.7 copy.85
  (63 shorter events, 3.3 us)
Async XLA Ops:
  0.0 26.3 %copy-start = (bf16[512,512]{1,0:T(8,128)(2,1)S(1)}, bf16[512,512]{1,0:T(8,128)(2,1)}, u32[]{:S(2)}) copy-start(bf16[512,512]{1,0:T(8,128)(2,1)} %param.27) | copy-start | bytes 1572868
  3.4 0.9 copy-start.12
  27.6 1.6 %copy-start.17 = (bf16[512,256]{1,0:T(8,128)(2,1)S(1)}, bf16[512,256]{1,0:T(8,128)(2,1)}, u32[]{:S(2)}) copy-start(bf16[512,256]{1,0:T(8,128)(2,1)} %param.25) | copy-start | bytes 786436
  32.2 2.4 %copy-start.21 = (bf16[512,512]{1,0:T(8,128)(2,1)S(1)}, bf16[512,512]{1,0:T(8,128)(2,1)}, u32[]{:S(2)}) copy-start(bf16[512,512]{1,0:T(8,128)(2,1)} %param.28) | copy-start | bytes 1572868
  35.6 1.0 copy-start.18
  37.3 1.6 %copy-start.1 = (bf16[512,2048]{1,0:T(8,128)(2,1)S(1)}, bf16[512,2048]{1,0:T(8,128)(2,1)}, u32[]{:S(2)}) copy-start(bf16[512,2048]{1,0:T(8,128)(2,1)} %pb_ref.1) | copy-start | bytes 6291460
  37.3 1.8 %copy-start.8 = (bf16[256,2048]{1,0:T(8,128)(2,1)S(1)}, bf16[256,2048]{1,0:T(8,128)(2,1)}, u32[]{:S(2)}) copy-start(bf16[256,2048]{1,0:T(8,128)(2,1)} %pa_ref.1) | copy-start | bytes 3145732
  39.2 2.5 %copy-start.13 = (bf16[48,2048]{1,0:T(8,128)(2,1)S(1)}, bf16[48,2048]{1,0:T(8,128)(2,1)}, u32[]{:S(2)}) copy-start(bf16[48,2048]{1,0:T(8,128)(2,1)} %base_ref.1) | copy-start | bytes 589828
  39.2 2.5 %copy-start.14 = (f32[2048]{0:T(1024)S(1)}, f32[2048]{0:T(1024)}, u32[]{:S(2)}) copy-start(f32[2048]{0:T(1024)} %param.31) | copy-start | bytes 24580
  39.2 19.7 %copy-start.19 = (s32[192,2]{0,1:T(2,128)S(1)}, s32[192,2]{0,1:T(2,128)}, u32[]{:S(2)}) copy-start(s32[192,2]{0,1:T(2,128)} %param.32) | copy-start | bytes 4612
  58.2 0.7 copy-start.10
  58.8 40.2 %copy-start.6 = (bf16[4,48,2048]{2,1,0:T(8,128)(2,1)}, bf16[4,48,2048]{2,1,0:T(8,128)(2,1)S(1)}, u32[]{:S(2)}) copy-start(bf16[4,48,2048]{2,1,0:T(8,128)(2,1)S(1)} %get-tuple-element.11) | copy-start | bytes 2359300
  92.7 1.6 %copy-start.15 = (bf16[1,2048,512]{2,1,0:T(8,128)(2,1)S(1)}, bf16[1,2048,512]{2,1,0:T(8,128)(2,1)}, u32[]{:S(2)}) copy-start(bf16[1,2048,512]{2,1,0:T(8,128)(2,1)} %param.37) | copy-start | bytes 6291460
  94.3 1.6 %copy-start.16 = (bf16[1,2048,512]{2,1,0:T(8,128)(2,1)S(1)}, bf16[1,2048,512]{2,1,0:T(8,128)(2,1)}, u32[]{:S(2)}) copy-start(bf16[1,2048,512]{2,1,0:T(8,128)(2,1)} %param.38) | copy-start | bytes 6291460
  95.9 3.2 %copy-start.2 = (bf16[1,512,2048]{2,1,0:T(8,128)(2,1)S(1)}, bf16[1,512,2048]{2,1,0:T(8,128)(2,1)}, u32[]{:S(2)}) copy-start(bf16[1,512,2048]{2,1,0:T(8,128)(2,1)} %param.39) | copy-start | bytes 6291460
  99.0 27.2 %copy-start.3 = (bf16[2048,512]{1,0:T(8,128)(2,1)S(1)}, bf16[2048,512]{1,0:T(8,128)(2,1)}, u32[]{:S(2)}) copy-start(bf16[2048,512]{1,0:T(8,128)(2,1)} %gate_ref.1) | copy-start | bytes 6291460
  99.0 27.2 %copy-start.4 = (bf16[2048,512]{1,0:T(8,128)(2,1)S(1)}, bf16[2048,512]{1,0:T(8,128)(2,1)}, u32[]{:S(2)}) copy-start(bf16[2048,512]{1,0:T(8,128)(2,1)} %up_ref.1) | copy-start | bytes 6291460
  99.1 27.2 %copy-start.7 = (bf16[4,48,2048]{2,1,0:T(8,128)(2,1)S(1)}, bf16[4,48,2048]{2,1,0:T(8,128)(2,1)}, u32[]{:S(2)}) copy-start(bf16[4,48,2048]{2,1,0:T(8,128)(2,1)} %copy-done.6) | copy-start | bytes 2359300
  126.2 1.6 %copy-start.20 = (f32[192,2]{0,1:T(2,128)S(1)}, f32[192,2]{0,1:T(2,128)}, u32[]{:S(2)}) copy-start(f32[192,2]{0,1:T(2,128)} %param.33) | copy-start | bytes 4612
  126.2 2.4 %copy-start.5 = (bf16[512,2048]{1,0:T(8,128)(2,1)S(1)}, bf16[512,2048]{1,0:T(8,128)(2,1)}, u32[]{:S(2)}) copy-start(bf16[512,2048]{1,0:T(8,128)(2,1)} %down_ref.1) | copy-start | bytes 6291460
  128.6 0.9 copy-start.9
  129.5 2.0 %copy-start.11 = (bf16[48,2048]{1,0:T(8,128)(2,1)S(1)}, bf16[48,2048]{1,0:T(8,128)(2,1)}, u32[]{:S(2)}) copy-start(bf16[48,2048]{1,0:T(8,128)(2,1)} %copy-done.10) | copy-start | bytes 589828
